TPU v7x, 32 devices: a whole 2x2x4 slice. The times are simulated.
32 devices in a mesh: grp: 2 (over x), ep: 16 (over z, y, core).
Axes of the slice: x: 2, y: 2, z: 4, core: 2. Of those that a mesh axis runs over, the one named last changes fastest.
Arguments:
- tokens: bfloat16 [8192, 2048], P(('grp', 'ep')), parts along dimension 0, may hold values from -6 to 6
- norm_gain: float32 [2048], replicated, may hold values from 0.1 to 1.9
- route_ids: int32 [8192, 2], P(('grp', 'ep')), parts along dimension 0, may hold values from 0 to 15, as said below
- route_slots: int32 [8192, 2], P(('grp', 'ep')), parts along dimension 0, may hold values from 0 to 47, as said below
- route_weights: float32 [8192, 2], P(('grp', 'ep')), parts along dimension 0, may hold values from 0.1 to 1
- w_gate: bfloat16 [16, 2048, 512], P('ep'), may hold values from -0.125 to 0.125
- w_up: bfloat16 [16, 2048, 512], P('ep'), may hold values from -0.125 to 0.125
- w_down: bfloat16 [16, 512, 2048], P('ep'), may hold values from -0.25 to 0.25
Outputs:
- expert_mix: bfloat16 [8192, 2048], P(('grp', 'ep')), parts along dimension 0
There are 2 independent parts, one for each index of `grp`. A program takes and returns all parts, laid end to end along the dimension named above; an argument that names none is the same for every part. Nothing has to cross between parts.
Inputs may be any that keep to these rules, and one draw needn't show every extreme that they name: `route_ids`: expert e belongs to group e // 4. Each token names 2 different experts of one group. In each aligned block of 256 tokens (the rows of one device) no expert is named more than 48 times, and some expert exactly 48 times. `route_slots`: in each aligned block of 256 tokens, the entries that name one expert hold distinct slots 0, 1, ... up to their count less one.
All inputs are finite; a program needn't handle non-finite values.
Results may differ from a plain program's by a relative error of at most 0.007.
Values may be sent and summed in bfloat16 or wider, within the bound.
A program may use at most 64 MiB of HBM per device.

v0:
```python
import functools

import jax
import jax.numpy as jnp
from jax import lax
from jax.experimental import pallas as pl
from jax.experimental.pallas import tpu as pltpu
from jax.sharding import PartitionSpec as P

GROUPS = 4
META = 128
CHUNKS = 4
SCHEDULE = (
    "P2", "P0", "D0", "P1", "P3", "H0", "H1", "H2", "H3", "C0", "D2", "D1", "C2", "D3", "M2", "C3", "C1", "M3", "M1", "M0",
)
NT = (((1,), (1,)), ((), ()))
F32 = jnp.float32
BF16 = jnp.bfloat16


def flip(index, bits):
    out, weight = index, 1
    while weight <= bits:
        if bits & weight:
            out = out + weight * (1 - 2 * ((index // weight) % 2))
        weight *= 2
    return out


def where01(hit):
    return jnp.where(hit, 1.0, 0.0).astype(BF16)


def iota(shape, dim):
    return lax.broadcasted_iota(jnp.int32, shape, dim)


def dot(a, b):
    return jnp.dot(a, b, preferred_element_type=F32)


def dot_nt(a, b):
    return lax.dot_general(a, b, NT, preferred_element_type=F32)


def kernel(
    peers, capp,
    tok, gain, ids, slots, wts, wg_hbm, wu_hbm, wd_hbm,
    out,
    normed, meta, n_out, n_in, spreads, picks, homes,
    x_out, x_in, y_out, e_in, hid, r_out, r_in, m_out, h_in, wg, wu, wd,
    w_sem, ns, nr, xs, xr, ys, yr, rs, rr, hs, hr,
):
    rows, feat = tok.shape
    ffn = wg.shape[1]
    block, width = x_out.shape[2:]
    chunks = feat // width
    spread = peers * capp
    me = lax.axis_index("ep")
    group, rank = me // peers, me % peers
    shift = peers.bit_length() - 1
    mesh_id = pl.DeviceIdType.MESH

    def at(d, j):
        return {"ep": flip(group, d) * peers + flip(rank, j)}

    barrier = pltpu.get_barrier_semaphore()
    for d in range(1, GROUPS):
        pl.semaphore_signal(barrier, inc=1, device_id=at(d, 0), device_id_type=mesh_id)
    for j in range(1, peers):
        pl.semaphore_signal(barrier, inc=1, device_id=at(0, j), device_id_type=mesh_id)

    loads = [
        pltpu.make_async_copy(src, dst, w_sem.at[i])
        for i, (src, dst) in enumerate(((wg_hbm, wg), (wu_hbm, wu), (wd_hbm, wd)))
    ]
    for load in loads:
        load.start()

    started = {}

    def send(key, src, dst, sent, got, where):
        copy = pltpu.make_async_remote_copy(
            src_ref=src, dst_ref=dst, send_sem=sent, recv_sem=got,
            device_id=where, device_id_type=mesh_id,
        )
        copy.start()
        started[key] = copy

    step = 32

    def norm_rows(i, carry):
        at_rows = pl.ds(pl.multiple_of(i * step, step), step)
        v = tok[at_rows, :].astype(F32)
        scale = lax.rsqrt(jnp.mean(v * v, axis=-1, keepdims=True) + 1e-06)
        normed[at_rows, :] = (v * scale * gain[...]).astype(BF16)
        return carry

    lax.fori_loop(0, rows // step, norm_rows, 0)

    tok_group = ids[0:1, :] >> shift
    member = where01(iota((16, rows), 0) == tok_group)
    before = dot(member, where01(iota((rows, rows), 0) < iota((rows, rows), 1)))
    place = jnp.sum(before * member.astype(F32), axis=0, keepdims=True)
    kind = iota((META, rows), 0)
    facts = jnp.where(kind == 8, tok_group.astype(F32), jnp.where(kind == 9, place, 0.0))
    for k in range(2):
        code = ((ids[k:k + 1, :] & (peers - 1)) ^ rank) * capp + slots[k:k + 1, :] + 1
        facts = jnp.where(kind == k, code.astype(F32), facts)
        w = wts[k:k + 1, :]
        for part in range(3):
            piece = w.astype(BF16).astype(F32)
            facts = jnp.where(kind == 2 + 3 * k + part, piece, facts)
            w = w - piece
    columns = dot_nt(where01(iota((rows, rows), 0) == iota((rows, rows), 1)), facts.astype(BF16))
    meta[...] = columns.astype(BF16)

    row_no = iota((block, rows), 0).astype(F32)
    tile = min(512, width)

    def tiles(width_of, body):
        def one(i, carry):
            body(pl.multiple_of(i * tile, tile))
            return carry

        lax.fori_loop(0, width_of // tile, one, 0)

    def pack(d):
        chosen = where01((row_no == place) & (tok_group == flip(group, d)))
        n_out[d] = dot(chosen, meta[...]).astype(BF16)
        if d:
            if len(started) == 0:
                pl.semaphore_wait(barrier, GROUPS - 1 + peers - 1)
            send(("n", d), n_out.at[d], n_in.at[d], ns.at[d], nr.at[d], at(d, 0))
        for c in range(chunks):
            def cols(t):
                x_out[d, c, :, pl.ds(t, tile)] = dot(chosen, normed[:, pl.ds(c * width + t, tile)]).astype(BF16)

            tiles(width, cols)
            if d:
                send(("x", d, c), x_out.at[d, c], x_in.at[d, c], xs.at[d, c], xr.at[d, c], at(d, 0))

    def part(j):
        return pl.ds(j * capp, capp)

    far_first = list(range(2, peers)) + [1]

    def dispatch(d):
        src, info = (x_in, n_in) if d else (x_out, n_out)
        if d:
            started["n", d].wait_recv()
        codes = dot_nt(where01(iota((16, META), 0) == iota((16, META), 1)), info[d])
        slot = (iota((spread, block), 0) + 1).astype(F32)
        spreads[d] = where01((slot == codes[0:1, :]) | (slot == codes[1:2, :]))
        for c in range(chunks):
            if d:
                started["x", d, c].wait_recv()

            def cols(t):
                got = dot(spreads[d], src[d, c, :, pl.ds(t, tile)]).astype(BF16)
                e_in[d, c, :capp, pl.ds(t, tile)] = got[:capp]
                y_out[d, c, capp:, pl.ds(t, tile)] = got[capp:]

            tiles(width, cols)
            for j in far_first:
                send(("y", d, c, j), y_out.at[d, c, part(j)], e_in.at[d, c, part(j)],
                     ys.at[d, c, j], yr.at[d, c, j], at(0, j))
        slot = (iota((block, spread), 1) + 1).astype(F32)
        about = info[d].astype(F32)
        for k in range(2):
            picks[d, k] = where01(slot == about[:, k:k + 1])

    def compute(d):
        if loads:
            for load in loads:
                load.wait()
            loads.clear()
        half = 256
        for c in range(chunks):
            for j in range(1, peers):
                started["y", d, c, j].wait_recv()

        def up(i, carry):
            f = pl.ds(pl.multiple_of(i * half, half), half)
            gate = sum(dot(e_in[d, c], wg[c * width:(c + 1) * width, f]) for c in range(chunks))
            upper = sum(dot(e_in[d, c], wu[c * width:(c + 1) * width, f]) for c in range(chunks))
            hid[:, f] = (gate / (1.0 + jnp.exp(-gate)) * upper).astype(BF16)
            return carry

        lax.fori_loop(0, ffn // half, up, 0)
        for c in range(chunks):
            def down(t):
                got = dot(hid[...], wd[:, pl.ds(c * width + t, tile)]).astype(BF16)
                r_in[d, c, :capp, pl.ds(t, tile)] = got[:capp]
                r_out[d, c, capp:, pl.ds(t, tile)] = got[capp:]

            tiles(width, down)
            for j in far_first:
                send(("r", d, c, j), r_out.at[d, c, part(j)], r_in.at[d, c, part(j)],
                     rs.at[d, c, j], rr.at[d, c, j], at(0, j))

    def combine(d):
        info = (n_in if d else n_out)[d].astype(F32)
        weigh = [info[:, b:b + 1] + info[:, b + 1:b + 2] + info[:, b + 2:b + 3] for b in (2, 5)]
        dst = m_out if d else h_in
        for c in range(chunks):
            for j in range(1, peers):
                started["r", d, c, j].wait_recv()

            def cols(t):
                got = r_in[d, c, :, pl.ds(t, tile)]
                mixed = weigh[0] * dot(picks[d, 0], got) + weigh[1] * dot(picks[d, 1], got)
                dst[d, c, :, pl.ds(t, tile)] = mixed.astype(BF16)

            tiles(width, cols)
            if d:
                send(("h", d, c), m_out.at[d, c], h_in.at[d, c], hs.at[d, c], hr.at[d, c], at(d, 0))

    def aim(d):
        slot = iota((rows, block), 1).astype(F32)
        homes[d] = where01((slot == columns[:, 9:10]) & (columns[:, 8:9] == flip(group, d).astype(F32)))

    stages = {"P": pack, "D": dispatch, "C": compute, "M": combine, "H": aim}
    for item in SCHEDULE:
        stages[item[0]](int(item[1]))

    for c in range(chunks):
        for d in range(1, GROUPS):
            started["h", d, c].wait_recv()

        def finish(t):
            total = dot(homes[0], h_in[0, c, :, pl.ds(t, tile)])
            for d in range(1, GROUPS):
                total += dot(homes[d], h_in[d, c, :, pl.ds(t, tile)])
            out[:, pl.ds(c * width + t, tile)] = total.astype(BF16)

        tiles(width, finish)
    for copy in started.values():
        copy.wait_send()


def shards(tokens, norm_gain, route_ids, route_slots, route_weights, w_gate, w_up, w_down):
    rows, feat = tokens.shape
    n_devices = lax.axis_size("ep")
    top_count = route_ids.shape[1]
    cap = 3 * top_count * rows // (2 * n_devices)
    capp = -(-cap // 16) * 16
    peers = n_devices // GROUPS
    block = peers * cap // top_count
    spread = peers * capp
    ffn = w_gate.shape[2]
    width = feat // CHUNKS
    vmem = pl.BlockSpec(memory_space=pltpu.VMEM)
    anywhere = pl.BlockSpec(memory_space=pl.ANY)
    dma = pltpu.SemaphoreType.DMA

    def buf(*shape):
        return pltpu.VMEM(shape, BF16)

    return pl.pallas_call(
        functools.partial(kernel, peers, capp),
        out_shape=jax.ShapeDtypeStruct((rows, feat), BF16),
        in_specs=[vmem] * 5 + [anywhere] * 3,
        out_specs=vmem,
        scratch_shapes=[
            buf(rows, feat), buf(rows, META),
            buf(GROUPS, block, META), buf(GROUPS, block, META),
            buf(GROUPS, spread, block), buf(GROUPS, 2, block, spread), buf(GROUPS, rows, block),
            buf(GROUPS, CHUNKS, block, width), buf(GROUPS, CHUNKS, block, width),
            buf(GROUPS, CHUNKS, spread, width), buf(GROUPS, CHUNKS, spread, width),
            buf(spread, ffn),
            buf(GROUPS, CHUNKS, spread, width), buf(GROUPS, CHUNKS, spread, width),
            buf(GROUPS, CHUNKS, block, width), buf(GROUPS, CHUNKS, block, width),
            buf(feat, ffn), buf(feat, ffn), buf(ffn, feat),
            dma((3,)),
            dma((GROUPS,)), dma((GROUPS,)),
            dma((GROUPS, CHUNKS)), dma((GROUPS, CHUNKS)),
            dma((GROUPS, CHUNKS, peers)), dma((GROUPS, CHUNKS, peers)),
            dma((GROUPS, CHUNKS, peers)), dma((GROUPS, CHUNKS, peers)),
            dma((GROUPS, CHUNKS)), dma((GROUPS, CHUNKS)),
        ],
        compiler_params=pltpu.CompilerParams(
            collective_id=0, has_side_effects=True, vmem_limit_bytes=60 * 1024 * 1024
        ),
    )(
        tokens, norm_gain.reshape(1, feat), route_ids.T, route_slots.T, route_weights.T,
        w_gate.reshape(feat, ffn), w_up.reshape(feat, ffn), w_down.reshape(ffn, feat),
    )


def solution(mesh):
    placed = (
        P(("grp", "ep"), None),
        P(),
        P(("grp", "ep"), None),
        P(("grp", "ep"), None),
        P(("grp", "ep"), None),
        P("ep", None, None),
        P("ep", None, None),
        P("ep", None, None),
    )
    return jax.shard_map(
        shards, mesh=mesh, in_specs=placed, out_specs=P(("grp", "ep"), None), check_vma=False
    )
```

profile of v0, /device:TPU:0, one launch (start us, length us, event | category | flops | bytes accessed | tf_op | source)
XLA Modules:
  0.0 95.9 jit_solution(6836609808366623453)
XLA Ops:
  0.0 93.6 %shard_map.82 = bf16[256,2048]{1,0:T(8,128)(2,1)} custom-call(bf16[256,2048]{1,0:T(8,128)(2,1)} %tok.1, f32[1,2048]{1,0:T(1,128)} %bitcast.10, s32[2,256]{1,0:T(2,128)} %bitcast.11, s32[2,256]{1,0:T(2,128)} %bitcast.12, f32[2,256]{1,0:T(2,128)} %bitcast.13, bf16[2048,512]{1,0:T(8,128)(2,1)} %bitcast.7, bf16[2048,512]{1,0:T(8,128)(2,1)} %bitcast.8, ...), custom_call_target="tpu_custom_call" | custom-call | tf_op jit(solution)/shard_map/pallas_call | solution.py:260
  93.6 2.3 %copy.10 = bf16[256,2048]{1,0:T(8,128)(2,1)} copy(bf16[256,2048]{1,0:T(8,128)(2,1)} %shard_map.82) | data formatting | bytes 2097152
where the time goes:
time: 96.1 us; the launch traced here: 95.9 us
  Pallas kernels  93.6 us (97%)
  local copies, waits for them, and re-layouts  2.3 us (2%)
    pallas_call x1, Pallas kernels, shards(): pl.pallas_call(functools.partial(kernel, peers, capp), out_shape=jax.Shap...  93.6 us
    unnamed x1, local copies, waits for them, and re-layouts  2.3 us

commit v1 on v0

v1 whole, which is shorter than its diff:
```python
import functools

import jax
import jax.numpy as jnp
from jax import lax
from jax.experimental import pallas as pl
from jax.experimental.pallas import tpu as pltpu
from jax.sharding import PartitionSpec as P

GROUPS = 4
FACTS = 16
LANES = 128
CHUNKS = 4
SCHEDULE = (
    "D10", "U00", "D11", "U01", "D12", "D20", "U02", "D13", "C0", "D21", "U10", "U11", "D22", "U12", "D23", "R00",
    "C1", "U20", "U21", "U22", "C2", "D30", "M20", "D31", "M21", "M22", "R10", "R11", "D32", "M23", "D33", "R12",
    "U30", "U31", "U32", "C3", "R13", "R01", "R02", "R03", "M30", "M31", "M32", "M33", "M10", "M11", "M12", "M13",
    "F0", "F1", "F2", "F3",
)
NT = (((1,), (1,)), ((), ()))
F32 = jnp.float32
BF16 = jnp.bfloat16


def flip(index, bits):
    out, weight = index, 1
    while weight <= bits:
        if bits & weight:
            out = out + weight * (1 - 2 * ((index // weight) % 2))
        weight *= 2
    return out


def where01(hit):
    return jnp.where(hit, 1.0, 0.0).astype(BF16)


def iota(shape, dim):
    return lax.broadcasted_iota(jnp.int32, shape, dim)


def dot(a, b):
    return jnp.dot(a, b, preferred_element_type=F32)


def dot_nt(a, b):
    return lax.dot_general(a, b, NT, preferred_element_type=F32)


def kernel(
    peers, capp,
    tok_hbm, gain_hbm, ids_hbm, slots_hbm, wts_hbm, wg_hbm, wu_hbm, wd_hbm,
    out,
    tok, gain, ids, slots, wts, wg, wu, wd,
    normed, chosen, n_out, n_in, about, spreads, picks, own_picks, homes, home_w,
    x_out, x_in, y_out, e_in, acc, hid, r_out, r_in, m_out, h_in,
    l_sem, w_sem, ns, nr, xs, xr, ys, yr, rs, rr, hs, hr,
):
    rows, feat = tok.shape
    ffn = wg.shape[1]
    block, width = x_out.shape[2:]
    spread = peers * capp
    me = lax.axis_index("ep")
    group, rank = me // peers, me % peers
    inner = (group % 2 + group // 2) % 2
    shift = peers.bit_length() - 1
    mesh_id = pl.DeviceIdType.MESH

    def at(d, j):
        return {"ep": flip(group, d) * peers + flip(rank, j)}

    order = [0, 2 - inner, 1 + inner, 3]

    barrier = pltpu.get_barrier_semaphore()
    for d in range(1, GROUPS):
        pl.semaphore_signal(barrier, inc=1, device_id=at(d, 0), device_id_type=mesh_id)
    for j in range(1, peers):
        pl.semaphore_signal(barrier, inc=1, device_id=at(0, j), device_id_type=mesh_id)

    def fetch(pairs, sem):
        copies = [pltpu.make_async_copy(src, dst, sem.at[i]) for i, (src, dst) in enumerate(pairs)]
        for copy in copies:
            copy.start()
        return copies

    small = fetch(
        ((ids_hbm, ids), (slots_hbm, slots), (wts_hbm, wts), (gain_hbm, gain), (tok_hbm, tok)), l_sem
    )

    def send(src, dst, sent, got, where):
        pltpu.make_async_remote_copy(
            src_ref=src, dst_ref=dst, send_sem=sent, recv_sem=got,
            device_id=where, device_id_type=mesh_id,
        ).start()

    def receive(dst, got):
        pltpu.make_async_remote_copy(
            src_ref=dst, dst_ref=dst, send_sem=xs.at[0], recv_sem=got,
            device_id=at(1, 0), device_id_type=mesh_id,
        ).wait_recv()

    for copy in small[:3]:
        copy.wait()
    tok_group = ids[0:1, :] >> shift
    member = where01(iota((16, rows), 0) == tok_group)
    before = dot(member, where01(iota((rows, rows), 0) < iota((rows, rows), 1)))
    place = jnp.sum(before * member.astype(F32), axis=0, keepdims=True)
    kind = iota((FACTS, rows), 0)
    facts = jnp.where(kind == 8, tok_group.astype(F32), jnp.where(kind == 9, place, 0.0))
    codes = []
    for k in range(2):
        code = ((ids[k:k + 1, :] & (peers - 1)) ^ rank) * capp + slots[k:k + 1, :] + 1
        codes.append(code)
        facts = jnp.where(kind == k, code.astype(F32), facts)
        w = wts[k:k + 1, :]
        for part in range(3):
            piece = w.astype(BF16).astype(F32)
            facts = jnp.where(kind == 2 + 3 * k + part, piece, facts)
            w = w - piece
    facts = facts.astype(BF16)
    slot = iota((spread, rows), 0) + 1
    chosen[:spread, :] = where01(((slot == codes[0]) | (slot == codes[1])) & (tok_group == group))
    row_no = iota((block, rows), 0).astype(F32)
    n_out[...] = jnp.zeros_like(n_out)
    for d in range(1, GROUPS):
        mine = where01((row_no == place) & (tok_group == flip(group, d)))
        chosen[spread + (d - 1) * block:spread + d * block, :] = mine
        n_out[d - 1, :, :block] = dot_nt(facts, mine).astype(BF16)

    for copy in small[3:]:
        copy.wait()
    loads = fetch(((wg_hbm, wg), (wu_hbm, wu), (wd_hbm, wd)), w_sem)
    step = 32

    def norm_rows(i, carry):
        at_rows = pl.ds(pl.multiple_of(i * step, step), step)
        v = tok[at_rows, :].astype(F32)
        scale = lax.rsqrt(jnp.mean(v * v, axis=-1, keepdims=True) + 1e-06)
        normed[at_rows, :] = (v * scale * gain[...]).astype(BF16)
        return carry

    lax.fori_loop(0, rows // step, norm_rows, 0, unroll=True)

    far_first = list(range(2, peers)) + [1]
    theirs = pl.ds(capp, spread - capp)

    def send_spread(s, c):
        d = order[s]
        for j in far_first:
            send(y_out.at[d, c, pl.ds((j - 1) * capp, capp)], e_in.at[d, c, pl.ds(j * capp, capp)],
                 ys.at[0], yr.at[d, c], at(0, j))

    def send_back(d, c):
        for j in far_first:
            send(r_out.at[d, c, pl.ds((j - 1) * capp, capp)], r_in.at[d, c, pl.ds(j * capp, capp)],
                 rs.at[0], rr.at[d, c], at(0, j))

    def send_group(d, c):
        send(x_out.at[d - 1, c], x_in.at[d - 1, c], xs.at[0], xr.at[d - 1, c], at(d, 0))

    for c in range(CHUNKS):
        got = dot(chosen[...], normed[:, c * width:(c + 1) * width]).astype(BF16)
        e_in[0, c, :capp, :] = got[:capp]
        y_out[0, c, :, :] = got[capp:spread]
        for d in range(1, GROUPS):
            x_out[d - 1, c, :, :] = got[spread + (d - 1) * block:spread + d * block]
        if c == 0:
            pl.semaphore_wait(barrier, GROUPS - 1 + peers - 1)
            for d in range(1, GROUPS):
                send(n_out.at[d - 1], n_in.at[d - 1], ns.at[0], nr.at[d - 1], at(d, 0))
        send_spread(0, c)
        send_group(1, c)
        if c == 0:
            send_group(2, c)
    for c in range(1, CHUNKS):
        send_group(2, c)
    for c in range(CHUNKS):
        send_group(3, c)

    columns = dot_nt(where01(iota((rows, rows), 0) == iota((rows, rows), 1)), facts)
    slot = (iota((rows, spread), 1) + 1).astype(F32)
    ours = columns[:, 8:9] == group.astype(F32)
    for k in range(2):
        own_picks[k] = where01((slot == columns[:, k:k + 1]) & ours)
        b = 2 + 3 * k
        home_w[k] = columns[:, b:b + 1] + columns[:, b + 1:b + 2] + columns[:, b + 2:b + 3]
    slot = iota((rows, block), 1).astype(F32)
    for d in range(1, GROUPS):
        homes[d - 1] = where01((slot == columns[:, 9:10]) & (columns[:, 8:9] == flip(group, d).astype(F32)))

    def dispatch(s, c):
        d = order[s]
        if c == 0:
            receive(n_in.at[d - 1], nr.at[d - 1])
            info = n_in[d - 1]
            code = info[:, :block].astype(F32)
            slot = (iota((spread, block), 0) + 1).astype(F32)
            spreads[d - 1] = where01((slot == code[0:1, :]) | (slot == code[1:2, :]))
        receive(x_in.at[d - 1, c], xr.at[d - 1, c])
        got = dot(spreads[d - 1], x_in[d - 1, c]).astype(BF16)
        e_in[d, c, :capp, :] = got[:capp]
        y_out[d, c, :, :] = got[capp:]
        send_spread(s, c)
        if c == CHUNKS - 1:
            info = n_in[d - 1]
            facts_of = dot_nt(where01(iota((block, LANES), 0) == iota((block, LANES), 1)), info)
            about[d - 1] = facts_of
            slot = (iota((block, spread), 1) + 1).astype(F32)
            for k in range(2):
                picks[d - 1, k] = where01(slot == facts_of[:, k:k + 1])

    half = min(256, ffn)

    def partial(s, c, w, f):
        return dot(e_in[order[s], c], w[c * width:(c + 1) * width, f])

    def gather(s, c):
        d = order[s]
        if loads:
            for load in loads:
                load.wait()
            loads.clear()
        receive(e_in.at[d, c, theirs], yr.at[d, c])
        if c < CHUNKS - 1:
            for i, w in enumerate((wg, wu)):
                for f in range(0, ffn, half):
                    f = slice(f, f + half)
                    if c == 0:
                        acc[d, i, :, f] = partial(s, c, w, f)
                    else:
                        acc[d, i, :, f] += partial(s, c, w, f)

    def compute(s):
        d, c = order[s], CHUNKS - 1
        gather(s, c)
        for f in range(0, ffn, half):
            f = slice(f, f + half)
            gate = acc[d, 0, :, f] + partial(s, c, wg, f)
            upper = acc[d, 1, :, f] + partial(s, c, wu, f)
            hid[:, f] = (gate / (1.0 + jnp.exp(-gate)) * upper).astype(BF16)
        for c in range(CHUNKS):
            got = dot(hid[...], wd[:, c * width:(c + 1) * width]).astype(BF16)
            r_in[d, c, :capp, :] = got[:capp]
            r_out[d, c, :, :] = got[capp:]
            if s > 1:
                send_back(s, c)

    def mix(d, c):
        facts_of = about[d - 1]
        weigh = [facts_of[:, b:b + 1] + facts_of[:, b + 1:b + 2] + facts_of[:, b + 2:b + 3] for b in (2, 5)]
        receive(r_in.at[d, c, theirs], rr.at[d, c])
        got = r_in[d, c]
        mixed = weigh[0] * dot(picks[d - 1, 0], got) + weigh[1] * dot(picks[d - 1, 1], got)
        m_out[d - 1, c, :, :] = mixed.astype(BF16)
        send(m_out.at[d - 1, c], h_in.at[d - 1, c], hs.at[0], hr.at[d - 1, c], at(d, 0))

    def finish(c):
        receive(r_in.at[0, c, theirs], rr.at[0, c])
        got = r_in[0, c]
        total = home_w[0] * dot(own_picks[0], got) + home_w[1] * dot(own_picks[1], got)
        for d in range(1, GROUPS):
            receive(h_in.at[d - 1, c], hr.at[d - 1, c])
        total += sum(dot(homes[d - 1], h_in[d - 1, c]) for d in range(1, GROUPS))
        out[:, c * width:(c + 1) * width] = total.astype(BF16)

    stages = {"D": dispatch, "U": gather, "C": compute, "R": send_back, "M": mix, "F": finish}
    for item in SCHEDULE:
        stages[item[0]](*(int(i) for i in item[1:]))

    for src, dst, sent, got in (
        (n_out, n_in, ns, nr), (x_out, x_in, xs, xr), (y_out, r_out, ys, yr), (r_out, y_out, rs, rr), (m_out, h_in, hs, hr),
    ):
        pltpu.make_async_remote_copy(
            src_ref=src, dst_ref=dst, send_sem=sent.at[0], recv_sem=got.at[(0,) * len(got.shape)],
            device_id=at(1, 0), device_id_type=mesh_id,
        ).wait_send()


def shards(tokens, norm_gain, route_ids, route_slots, route_weights, w_gate, w_up, w_down):
    rows, feat = tokens.shape
    n_devices = lax.axis_size("ep")
    top_count = route_ids.shape[1]
    cap = 3 * top_count * rows // (2 * n_devices)
    capp = -(-cap // 16) * 16
    peers = n_devices // GROUPS
    block = peers * cap // top_count
    spread = peers * capp
    ffn = w_gate.shape[2]
    width = feat // CHUNKS
    others = GROUPS - 1
    anywhere = pl.BlockSpec(memory_space=pl.ANY)
    vmem = pl.BlockSpec(memory_space=pltpu.VMEM)
    dma = pltpu.SemaphoreType.DMA

    def buf(*shape, kind=BF16):
        return pltpu.VMEM(shape, kind)

    return pl.pallas_call(
        functools.partial(kernel, peers, capp),
        out_shape=pltpu.VMEM((rows, feat), BF16),
        in_specs=[anywhere] * 8,
        out_specs=vmem,
        scratch_shapes=[
            buf(rows, feat), buf(1, feat, kind=F32), buf(top_count, rows, kind=jnp.int32),
            buf(top_count, rows, kind=jnp.int32), buf(top_count, rows, kind=F32),
            buf(feat, ffn), buf(feat, ffn), buf(ffn, feat),
            buf(rows, feat), buf(spread + others * block, rows),
            buf(others, FACTS, LANES), buf(others, FACTS, LANES), buf(others, block, FACTS, kind=F32),
            buf(others, spread, block), buf(others, 2, block, spread), buf(2, rows, spread),
            buf(others, rows, block), buf(2, rows, 1, kind=F32),
            buf(others, CHUNKS, block, width), buf(others, CHUNKS, block, width),
            buf(GROUPS, CHUNKS, spread - capp, width), buf(GROUPS, CHUNKS, spread, width),
            buf(GROUPS, 2, spread, ffn, kind=F32), buf(spread, ffn),
            buf(GROUPS, CHUNKS, spread - capp, width), buf(GROUPS, CHUNKS, spread, width),
            buf(others, CHUNKS, block, width), buf(others, CHUNKS, block, width),
            dma((5,)), dma((3,)),
            dma((1,)), dma((others,)),
            dma((1,)), dma((others, CHUNKS)),
            dma((1,)), dma((GROUPS, CHUNKS)),
            dma((1,)), dma((GROUPS, CHUNKS)),
            dma((1,)), dma((others, CHUNKS)),
        ],
        compiler_params=pltpu.CompilerParams(
            collective_id=0, has_side_effects=True, vmem_limit_bytes=60 * 1024 * 1024
        ),
    )(
        tokens, norm_gain.reshape(1, feat), route_ids.T, route_slots.T, route_weights.T,
        w_gate.reshape(feat, ffn), w_up.reshape(feat, ffn), w_down.reshape(ffn, feat),
    )


def solution(mesh):
    placed = (
        P(("grp", "ep"), None),
        P(),
        P(("grp", "ep"), None),
        P(("grp", "ep"), None),
        P(("grp", "ep"), None),
        P("ep", None, None),
        P("ep", None, None),
        P("ep", None, None),
    )
    return jax.shard_map(
        shards, mesh=mesh, in_specs=placed, out_specs=P(("grp", "ep"), None), check_vma=False
    )
```

time: 96.1 us -> 88.6 us (0.922)
  Pallas kernels: 93.6 us -> 87.5 us
  local copies, waits for them, and re-layouts: 2.3 us -> 0.97 us
    pallas_call x1, Pallas kernels: 93.6 us -> 87.5 us  [shards(): pl.pallas_call(functools.partial(kernel, peers, capp), out_shape=pltpu.VM...]
    unnamed x1, local copies, waits for them, and re-layouts: 2.3 us -> 0.97 us
where the time goes in v1:
time: 88.6 us; the launch traced here: 88.5 us
  Pallas kernels  87.5 us (99%)
  local copies, waits for them, and re-layouts  0.97 us (1%)
    pallas_call x1, Pallas kernels, shards(): pl.pallas_call(functools.partial(kernel, peers, capp), out_shape=pltpu.VM...  87.5 us

profile of v1, /device:TPU:0, one launch (start us, length us, event | category | flops | bytes accessed | tf_op | source)
XLA Modules:
  0.0 88.5 jit_solution(14311307480005152535)
XLA Ops:
  0.0 87.5 %shard_map.82 = bf16[256,2048]{1,0:T(8,128)(2,1)S(1)} custom-call(bf16[256,2048]{1,0:T(8,128)(2,1)} %tok_hbm.1, f32[1,2048]{1,0:T(1,128)} %bitcast.10, s32[2,256]{1,0:T(2,128)} %bitcast.11, s32[2,256]{1,0:T(2,128)} %bitcast.12, f32[2,256]{1,0:T(2,128)} %bitcast.13, bf16[2048,512]{1,0:T(8,128)(2,1)} %bitcast.7, bf16[2048,512]{1,0:T(8,128)(2,1)} %bitcast.8, ...), custom_call_target="tpu_custom_call" | custom-call | tf_op jit(solution)/shard_map/pallas_call | solution.py:298
  87.5 1.0 %copy.10 = bf16[256,2048]{1,0:T(8,128)(2,1)} copy(bf16[256,2048]{1,0:T(8,128)(2,1)S(1)} %shard_map.82) | data formatting | bytes 2097152

commit v2 on v1

--- a/solution.py
+++ b/solution.py
@@ -12,10 +12,10 @@
 LANES = 128
 CHUNKS = 4
 SCHEDULE = (
-    "D10", "U00", "D11", "U01", "D12", "D20", "U02", "D13", "C0", "D21", "U10", "U11", "D22", "U12", "D23", "R00",
-    "C1", "U20", "U21", "U22", "C2", "D30", "M20", "D31", "M21", "M22", "R10", "R11", "D32", "M23", "D33", "R12",
-    "U30", "U31", "U32", "C3", "R13", "R01", "R02", "R03", "M30", "M31", "M32", "M33", "M10", "M11", "M12", "M13",
-    "F0", "F1", "F2", "F3",
+    "D10", "U00", "D11", "U01", "D12", "X", "D20", "U02", "D13", "C0", "D21", "U10", "U11", "D22", "U12", "D23",
+    "R00", "C1", "U20", "U21", "U22", "C2", "D30", "M20", "D31", "M21", "D32", "M22", "M23", "D33", "R10", "U30",
+    "U31", "U32", "C3", "R11", "R12", "R13", "R01", "R02", "R03", "M10", "M30", "M31", "M32", "M33", "M11", "M12",
+    "M13", "F0", "F1", "F2", "F3",
 )
 NT = (((1,), (1,)), ((), ()))
 F32 = jnp.float32
@@ -170,12 +170,10 @@
                 send(n_out.at[d - 1], n_in.at[d - 1], ns.at[0], nr.at[d - 1], at(d, 0))
         send_spread(0, c)
         send_group(1, c)
-        if c == 0:
+
+        @pl.when(inner == 1)
+        def _():
             send_group(2, c)
-    for c in range(1, CHUNKS):
-        send_group(2, c)
-    for c in range(CHUNKS):
-        send_group(3, c)
 
     columns = dot_nt(where01(iota((rows, rows), 0) == iota((rows, rows), 1)), facts)
     slot = (iota((rows, spread), 1) + 1).astype(F32)
@@ -209,6 +207,15 @@
             for k in range(2):
                 picks[d - 1, k] = where01(slot == facts_of[:, k:k + 1])
 
+    def send_far():
+        @pl.when(inner == 0)
+        def _():
+            for c in range(CHUNKS):
+                send_group(2, c)
+
+        for c in range(CHUNKS):
+            send_group(3, c)
+
     half = min(256, ffn)
 
     def partial(s, c, w, f):
@@ -263,7 +270,7 @@
         total += sum(dot(homes[d - 1], h_in[d - 1, c]) for d in range(1, GROUPS))
         out[:, c * width:(c + 1) * width] = total.astype(BF16)
 
-    stages = {"D": dispatch, "U": gather, "C": compute, "R": send_back, "M": mix, "F": finish}
+    stages = {"X": send_far, "D": dispatch, "U": gather, "C": compute, "R": send_back, "M": mix, "F": finish}
     for item in SCHEDULE:
         stages[item[0]](*(int(i) for i in item[1:]))
 

time: 88.6 us -> 77.7 us (0.88)
  Pallas kernels: 87.5 us -> 76.6 us
    pallas_call x1, Pallas kernels: 87.5 us -> 76.6 us  [shards(): pl.pallas_call(functools.partial(kernel, peers, capp), out_shape=pltpu.VM...]
where the time goes in v2:
time: 77.7 us; the launch traced here: 77.5 us
  Pallas kernels  76.6 us (99%)
  local copies, waits for them, and re-layouts  0.97 us (1%)
    pallas_call x1, Pallas kernels, shards(): pl.pallas_call(functools.partial(kernel, peers, capp), out_shape=pltpu.VM...  76.6 us

profile of v2, /device:TPU:0, one launch (start us, length us, event | category | flops | bytes accessed | tf_op | source)
XLA Modules:
  0.0 77.5 jit_solution(10867620904781379969)
XLA Ops:
  0.0 76.6 %shard_map.82 = bf16[256,2048]{1,0:T(8,128)(2,1)S(1)} custom-call(bf16[256,2048]{1,0:T(8,128)(2,1)} %tok_hbm.1, f32[1,2048]{1,0:T(1,128)} %bitcast.10, s32[2,256]{1,0:T(2,128)} %bitcast.11, s32[2,256]{1,0:T(2,128)} %bitcast.12, f32[2,256]{1,0:T(2,128)} %bitcast.13, bf16[2048,512]{1,0:T(8,128)(2,1)} %bitcast.7, bf16[2048,512]{1,0:T(8,128)(2,1)} %bitcast.8, ...), custom_call_target="tpu_custom_call" | custom-call | tf_op jit(solution)/shard_map/pallas_call | solution.py:305
  76.6 1.0 %copy.10 = bf16[256,2048]{1,0:T(8,128)(2,1)} copy(bf16[256,2048]{1,0:T(8,128)(2,1)S(1)} %shard_map.82) | data formatting | bytes 2097152

commit v3 on v2

--- a/solution.py
+++ b/solution.py
@@ -11,11 +11,13 @@
 FACTS = 16
 LANES = 128
 CHUNKS = 4
+HELD = 2
+NEAR_FIRST = 2
 SCHEDULE = (
     "D10", "U00", "D11", "U01", "D12", "X", "D20", "U02", "D13", "C0", "D21", "U10", "U11", "D22", "U12", "D23",
-    "R00", "C1", "U20", "U21", "U22", "C2", "D30", "M20", "D31", "M21", "D32", "M22", "M23", "D33", "R10", "U30",
-    "U31", "U32", "C3", "R11", "R12", "R13", "R01", "R02", "R03", "M10", "M30", "M31", "M32", "M33", "M11", "M12",
-    "M13", "F0", "F1", "F2", "F3",
+    "Q000", "C1", "Q110", "U20", "U21", "U22", "C2", "D30", "M20", "D31", "M21", "D32", "M22", "N", "D33", "M23",
+    "Q010", "B0", "U30", "U31", "U32", "C3", "B1", "Q100", "R01", "R02", "R03", "L0", "L1", "L2", "L3", "L4",
+    "L5", "L6", "L7", "F0", "F1", "F2", "F3",
 )
 NT = (((1,), (1,)), ((), ()))
 F32 = jnp.float32
@@ -52,9 +54,9 @@
     tok_hbm, gain_hbm, ids_hbm, slots_hbm, wts_hbm, wg_hbm, wu_hbm, wd_hbm,
     out,
     tok, gain, ids, slots, wts, wg, wu, wd,
-    normed, chosen, n_out, n_in, about, spreads, picks, own_picks, homes, home_w,
+    earlier, normed, chosen, n_out, n_in, about, spreads, picks, own_picks, homes, home_w,
     x_out, x_in, y_out, e_in, acc, hid, r_out, r_in, m_out, h_in,
-    l_sem, w_sem, ns, nr, xs, xr, ys, yr, rs, rr, hs, hr,
+    ready, l_sem, w_sem, ns, nr, xs, xr, ys, yr, rs, rr, hs, hr,
 ):
     rows, feat = tok.shape
     ffn = wg.shape[1]
@@ -73,7 +75,9 @@
 
     barrier = pltpu.get_barrier_semaphore()
     for d in range(1, GROUPS):
-        pl.semaphore_signal(barrier, inc=1, device_id=at(d, 0), device_id_type=mesh_id)
+        @pl.when(flip(group, d) > 0)
+        def _():
+            pl.semaphore_signal(barrier, inc=1, device_id=at(d, 0), device_id_type=mesh_id)
     for j in range(1, peers):
         pl.semaphore_signal(barrier, inc=1, device_id=at(0, j), device_id_type=mesh_id)
 
@@ -99,11 +103,13 @@
             device_id=at(1, 0), device_id_type=mesh_id,
         ).wait_recv()
 
+    earlier[...] = where01(iota((rows, rows), 0) < iota((rows, rows), 1))
+    n_out[...] = jnp.zeros_like(n_out)
     for copy in small[:3]:
         copy.wait()
     tok_group = ids[0:1, :] >> shift
     member = where01(iota((16, rows), 0) == tok_group)
-    before = dot(member, where01(iota((rows, rows), 0) < iota((rows, rows), 1)))
+    before = dot(member, earlier[...])
     place = jnp.sum(before * member.astype(F32), axis=0, keepdims=True)
     kind = iota((FACTS, rows), 0)
     facts = jnp.where(kind == 8, tok_group.astype(F32), jnp.where(kind == 9, place, 0.0))
@@ -121,11 +127,9 @@
     slot = iota((spread, rows), 0) + 1
     chosen[:spread, :] = where01(((slot == codes[0]) | (slot == codes[1])) & (tok_group == group))
     row_no = iota((block, rows), 0).astype(F32)
-    n_out[...] = jnp.zeros_like(n_out)
     for d in range(1, GROUPS):
         mine = where01((row_no == place) & (tok_group == flip(group, d)))
         chosen[spread + (d - 1) * block:spread + d * block, :] = mine
-        n_out[d - 1, :, :block] = dot_nt(facts, mine).astype(BF16)
 
     for copy in small[3:]:
         copy.wait()
@@ -157,6 +161,22 @@
 
     def send_group(d, c):
         send(x_out.at[d - 1, c], x_in.at[d - 1, c], xs.at[0], xr.at[d - 1, c], at(d, 0))
+
+    def enter():
+        @pl.when(group == 0)
+        def _():
+            pl.semaphore_wait(barrier, peers - 1)
+
+        @pl.when(group > 0)
+        def _():
+            pl.semaphore_wait(barrier, GROUPS - 1 + peers - 1)
+        for g in range(1, GROUPS):
+            @pl.when(group == g)
+            def _():
+                pl.semaphore_signal(ready.at[g - 1], inc=1, device_id=at(g, 0), device_id_type=mesh_id)
+
+    def send_facts(d):
+        send(n_out.at[d - 1], n_in.at[d - 1], ns.at[0], nr.at[d - 1], at(d, 0))
 
     for c in range(CHUNKS):
         got = dot(chosen[...], normed[:, c * width:(c + 1) * width]).astype(BF16)
@@ -165,15 +185,33 @@
         for d in range(1, GROUPS):
             x_out[d - 1, c, :, :] = got[spread + (d - 1) * block:spread + d * block]
         if c == 0:
-            pl.semaphore_wait(barrier, GROUPS - 1 + peers - 1)
+            enter()
+        send_spread(0, c)
+
+        @pl.when(group > 0)
+        def _():
+            send_group(1, c)
+
+        @pl.when(inner == 1)
+        def _():
+            send_group(2, c)
+
+        if c == 0:
             for d in range(1, GROUPS):
-                send(n_out.at[d - 1], n_in.at[d - 1], ns.at[0], nr.at[d - 1], at(d, 0))
-        send_spread(0, c)
-        send_group(1, c)
-
-        @pl.when(inner == 1)
-        def _():
-            send_group(2, c)
+                mine = chosen[spread + (d - 1) * block:spread + d * block, :]
+                n_out[d - 1, :, :block] = dot_nt(facts, mine).astype(BF16)
+
+            @pl.when(group > 0)
+            def _():
+                for d in range(1, GROUPS):
+                    send_facts(d)
+
+    @pl.when(group == 0)
+    def _():
+        pl.semaphore_wait(ready.at[0], 1)
+        send_facts(1)
+        for c in range(CHUNKS):
+            send_group(1, c)
 
     columns = dot_nt(where01(iota((rows, rows), 0) == iota((rows, rows), 1)), facts)
     slot = (iota((rows, spread), 1) + 1).astype(F32)
@@ -184,7 +222,8 @@
         home_w[k] = columns[:, b:b + 1] + columns[:, b + 1:b + 2] + columns[:, b + 2:b + 3]
     slot = iota((rows, block), 1).astype(F32)
     for d in range(1, GROUPS):
-        homes[d - 1] = where01((slot == columns[:, 9:10]) & (columns[:, 8:9] == flip(group, d).astype(F32)))
+        there = where01((slot == columns[:, 9:10]) & (columns[:, 8:9] == flip(group, d).astype(F32)))
+        homes[:, (d - 1) * block:d * block] = there
 
     def dispatch(s, c):
         d = order[s]
@@ -208,6 +247,12 @@
                 picks[d - 1, k] = where01(slot == facts_of[:, k:k + 1])
 
     def send_far():
+        @pl.when(group == 0)
+        def _():
+            for d in (2, 3):
+                pl.semaphore_wait(ready.at[d - 1], 1)
+                send_facts(d)
+
         @pl.when(inner == 0)
         def _():
             for c in range(CHUNKS):
@@ -252,30 +297,70 @@
             if s > 1:
                 send_back(s, c)
 
-    def mix(d, c):
+    def mix(d, c, held=False):
         facts_of = about[d - 1]
         weigh = [facts_of[:, b:b + 1] + facts_of[:, b + 1:b + 2] + facts_of[:, b + 2:b + 3] for b in (2, 5)]
         receive(r_in.at[d, c, theirs], rr.at[d, c])
         got = r_in[d, c]
         mixed = weigh[0] * dot(picks[d - 1, 0], got) + weigh[1] * dot(picks[d - 1, 1], got)
         m_out[d - 1, c, :, :] = mixed.astype(BF16)
-        send(m_out.at[d - 1, c], h_in.at[d - 1, c], hs.at[0], hr.at[d - 1, c], at(d, 0))
+        if isinstance(d, int) and d == 2 and c < HELD:
+            pl.when(inner == 1)(functools.partial(send_home, d, c, flip(group, d)))
+        elif isinstance(d, int):
+            send_home(d, c, flip(group, d))
+        else:
+            send_home(d, c, choose(1 - (d - 1) // 2, flip(group, 3), flip(group, 1)))
+
+    def send_home(d, c, there):
+        send(m_out.at[d - 1, c], h_in.at[c, d - 1], hs.at[0], hr.at[c], {"ep": there * peers + rank})
+
+    def send_held():
+        @pl.when(inner == 0)
+        def _():
+            for c in range(HELD):
+                send_home(2, c, flip(group, 2))
+
+    def choose(which, a, b):
+        return a + which * (b - a)
+
+    def last_with(first):
+        near = [(1, c) for c in range(CHUNKS)]
+        return near[:first] + [(3, c) for c in range(CHUNKS)] + near[first:]
+
+    last, last_inner = last_with(1), last_with(NEAR_FIRST)
+
+    def mix_last(i):
+        mix(*(choose(inner, a, b) for a, b in zip(last[i], last_inner[i])))
+
+    def send_back_if(which, d, c):
+        pl.when(inner == which)(functools.partial(send_back, d, c))
+
+    def near_back(late):
+        @pl.when(inner == 1)
+        def _():
+            for c in range(NEAR_FIRST, CHUNKS) if late else range(1, NEAR_FIRST):
+                send_back(1, c)
+
+        if late:
+            @pl.when(inner == 0)
+            def _():
+                for c in range(1, CHUNKS):
+                    send_back(1, c)
 
     def finish(c):
+        receive(h_in.at[c], hr.at[c])
+        total = dot(homes[...], h_in[c].reshape(homes.shape[1], width))
         receive(r_in.at[0, c, theirs], rr.at[0, c])
         got = r_in[0, c]
-        total = home_w[0] * dot(own_picks[0], got) + home_w[1] * dot(own_picks[1], got)
-        for d in range(1, GROUPS):
-            receive(h_in.at[d - 1, c], hr.at[d - 1, c])
-        total += sum(dot(homes[d - 1], h_in[d - 1, c]) for d in range(1, GROUPS))
+        total += home_w[0] * dot(own_picks[0], got) + home_w[1] * dot(own_picks[1], got)
         out[:, c * width:(c + 1) * width] = total.astype(BF16)
 
-    stages = {"X": send_far, "D": dispatch, "U": gather, "C": compute, "R": send_back, "M": mix, "F": finish}
+    stages = {"X": send_far, "N": send_held, "D": dispatch, "U": gather, "C": compute, "R": send_back, "M": mix, "L": mix_last, "B": near_back, "Q": send_back_if, "F": finish}
     for item in SCHEDULE:
         stages[item[0]](*(int(i) for i in item[1:]))
 
     for src, dst, sent, got in (
-        (n_out, n_in, ns, nr), (x_out, x_in, xs, xr), (y_out, r_out, ys, yr), (r_out, y_out, rs, rr), (m_out, h_in, hs, hr),
+        (n_out, n_in, ns, nr), (x_out, x_in, xs, xr), (y_out, r_out, ys, yr), (r_out, y_out, rs, rr), (m_out, m_out, hs, hr),
     ):
         pltpu.make_async_remote_copy(
             src_ref=src, dst_ref=dst, send_sem=sent.at[0], recv_sem=got.at[(0,) * len(got.shape)],
@@ -311,21 +396,21 @@
             buf(rows, feat), buf(1, feat, kind=F32), buf(top_count, rows, kind=jnp.int32),
             buf(top_count, rows, kind=jnp.int32), buf(top_count, rows, kind=F32),
             buf(feat, ffn), buf(feat, ffn), buf(ffn, feat),
-            buf(rows, feat), buf(spread + others * block, rows),
+            buf(rows, rows), buf(rows, feat), buf(spread + others * block, rows),
             buf(others, FACTS, LANES), buf(others, FACTS, LANES), buf(others, block, FACTS, kind=F32),
             buf(others, spread, block), buf(others, 2, block, spread), buf(2, rows, spread),
-            buf(others, rows, block), buf(2, rows, 1, kind=F32),
+            buf(rows, others * block), buf(2, rows, 1, kind=F32),
             buf(others, CHUNKS, block, width), buf(others, CHUNKS, block, width),
             buf(GROUPS, CHUNKS, spread - capp, width), buf(GROUPS, CHUNKS, spread, width),
             buf(GROUPS, 2, spread, ffn, kind=F32), buf(spread, ffn),
             buf(GROUPS, CHUNKS, spread - capp, width), buf(GROUPS, CHUNKS, spread, width),
-            buf(others, CHUNKS, block, width), buf(others, CHUNKS, block, width),
-            dma((5,)), dma((3,)),
+            buf(others, CHUNKS, block, width), buf(CHUNKS, others, block, width),
+            pltpu.SemaphoreType.REGULAR((GROUPS - 1,)), dma((5,)), dma((3,)),
             dma((1,)), dma((others,)),
             dma((1,)), dma((others, CHUNKS)),
             dma((1,)), dma((GROUPS, CHUNKS)),
             dma((1,)), dma((GROUPS, CHUNKS)),
-            dma((1,)), dma((others, CHUNKS)),
+            dma((1,)), dma((CHUNKS,)),
         ],
         compiler_params=pltpu.CompilerParams(
             collective_id=0, has_side_effects=True, vmem_limit_bytes=60 * 1024 * 1024

time: 77.7 us -> 76.8 us (0.988)
  Pallas kernels: 76.6 us -> 75.6 us
    pallas_call x1, Pallas kernels: 76.6 us -> 75.6 us  [shards(): pl.pallas_call(functools.partial(kernel, peers, capp), out_shape=pltpu.VM...]
where the time goes in v3:
time: 76.8 us; the launch traced here: 76.6 us
  Pallas kernels  75.6 us (98%)
  local copies, waits for them, and re-layouts  0.97 us (1%)
    pallas_call x1, Pallas kernels, shards(): pl.pallas_call(functools.partial(kernel, peers, capp), out_shape=pltpu.VM...  75.6 us

profile of v3, /device:TPU:0, one launch (start us, length us, event | category | flops | bytes accessed | tf_op | source)
XLA Modules:
  0.0 76.6 jit_solution(16965394518493322884)
XLA Ops:
  0.0 75.6 %shard_map.82 = bf16[256,2048]{1,0:T(8,128)(2,1)S(1)} custom-call(bf16[256,2048]{1,0:T(8,128)(2,1)} %tok_hbm.1, f32[1,2048]{1,0:T(1,128)} %bitcast.10, s32[2,256]{1,0:T(2,128)} %bitcast.11, s32[2,256]{1,0:T(2,128)} %bitcast.12, f32[2,256]{1,0:T(2,128)} %bitcast.13, bf16[2048,512]{1,0:T(8,128)(2,1)} %bitcast.7, bf16[2048,512]{1,0:T(8,128)(2,1)} %bitcast.8, ...), custom_call_target="tpu_custom_call" | custom-call | tf_op jit(solution)/shard_map/pallas_call | solution.py:390
  75.6 1.0 %copy.10 = bf16[256,2048]{1,0:T(8,128)(2,1)} copy(bf16[256,2048]{1,0:T(8,128)(2,1)S(1)} %shard_map.82) | data formatting | bytes 2097152
